TPU v7x, 32 devices: a whole 2x2x4 slice. The times are simulated.
32 devices in a mesh: ep: 8 (over z, core), tp: 4 (over y, x).
Axes of the slice: x: 2, y: 2, z: 4, core: 2. Of those that a mesh axis runs over, the one named last changes fastest.
Arguments:
- mixer_input: bfloat16 [2048, 1024], P('ep', 'tp'), may hold values from -6 to 6
- log_step: float32 [64], P('tp'), may hold values from -12.8 to -2.7
- decay_shift: float32 [2048, 64], P('ep', 'tp'), may hold values from -2 to 0
- input_map: bfloat16 [2, 64, 64, 16], P(None, 'tp'), may hold values from -71.55418 to 71.55418
- readout: float32 [2, 64, 16, 64], P(None, 'tp'), may hold values from -0.5 to 0.5
- mixer_weight: bfloat16 [1024, 2048], P(None, 'tp'), may hold values from -0.1875 to 0.1875
- expert_input: bfloat16 [1024, 2048], P('ep'), may hold values from -6 to 6
- norm_gain: float32 [2048], replicated, may hold values from 0.1 to 1.9
- routes: int32 [1024, 2], P('ep'), may hold values from 0 to 7, all different within a row; in each aligned block of 128 rows (0 to 127, 128 to 255, ...) at most 64 rows name the same one
- route_weight: float32 [1024, 2], P('ep'), may hold values from 0.1 to 2.5
- expert_switch_matrix: bfloat16 [8, 2048, 4096], P('ep', None, 'tp'), may hold values from -0.125 to 0.125
- up_weight: bfloat16 [8, 2048, 4096], P('ep', None, 'tp'), may hold values from -0.125 to 0.125
- down_weight: bfloat16 [8, 4096, 2048], P('ep', None, 'tp'), may hold values from -0.09375 to 0.09375
- shared_gate: bfloat16 [2048, 1024], P(None, 'tp'), may hold values from -0.125 to 0.125
- shared_up: bfloat16 [2048, 1024], P(None, 'tp'), may hold values from -0.125 to 0.125
- shared_down: bfloat16 [1024, 2048], P(None, 'tp'), may hold values from -0.1875 to 0.1875
Outputs:
- mixer_out: bfloat16 [2048, 2048], P('ep', 'tp')
- experts_out: bfloat16 [1024, 2048], P('ep', 'tp')
Inputs may be any that keep to these rules, and one draw needn't show every extreme that they name: `routes`: each row names 2 different experts. In each aligned block of 128 rows (the rows of one index of ep) no expert is named by more than 64 rows, and in some block one expert is named by exactly 64 rows.
All inputs are finite; a program needn't handle non-finite values.
Results may differ from a plain program's by a relative error of at most 0.0069.
Values may be sent and summed in bfloat16 or wider, within the bound.
A program may use at most 128 MiB of HBM per device.

v0:
```python
import jax
import jax.numpy as jnp
from jax import lax
from jax.sharding import PartitionSpec as P


def carried_in(part, axis, combine, identity):
    place = lax.axis_index(axis)
    gathered = jax.tree.map(lambda a: lax.all_gather(a, axis), part)
    state = jax.tree.map(lambda a, e: jnp.zeros_like(a) + jnp.asarray(e, a.dtype), part, identity)

    def one(lap, state):
        return combine(
            state, jax.tree.map(lambda a: lax.dynamic_index_in_dim(a, lap, 0, False), gathered)
        )

    return lax.fori_loop(0, place, one, state)


def combine_parts(earlier, later):
    early_real, early_imaginary, early_shift_real, early_shift_imaginary = earlier
    late_real, late_imaginary, late_shift_real, late_shift_imaginary = later
    joint_real = late_real * early_real - late_imaginary * early_imaginary
    joint_imaginary = late_real * early_imaginary + late_imaginary * early_real
    shift_real = (
        late_real * early_shift_real - late_imaginary * early_shift_imaginary + late_shift_real
    )
    shift_imaginary = (
        late_real * early_shift_imaginary + late_imaginary * early_shift_real + late_shift_imaginary
    )
    return (joint_real, joint_imaginary, shift_real, shift_imaginary)


def factors(log_step, states):
    step_rate = jnp.exp(log_step)
    frequency = jnp.pi * jnp.arange(states, dtype=jnp.float32)
    angle = step_rate[:, None] * frequency[None, :]
    turn_cosine = jnp.cos(angle)
    turn_sine = jnp.sin(angle)
    base = jnp.exp(-0.5 * step_rate)[:, None]
    base_real = base * turn_cosine
    starting_quadrature = base * turn_sine
    inverse = 1.0 / (0.25 + frequency * frequency)[None, :]
    lowered = base_real - 1.0
    inject_real = (-0.5 * lowered + starting_quadrature * frequency[None, :]) * inverse
    inject_imaginary = (-0.5 * starting_quadrature - lowered * frequency[None, :]) * inverse
    return (step_rate, turn_cosine, turn_sine, inject_real, inject_imaginary)


def shards(
    mixer_input,
    log_step,
    decay_shift,
    input_map,
    readout,
    mixer_weight,
    expert_input,
    norm_gain,
    routes,
    route_weight,
    expert_switch_matrix,
    up_weight,
    down_weight,
    shared_gate,
    shared_up,
    shared_down,
):
    highest = lax.Precision.HIGHEST
    row_count = mixer_input.shape[0]
    groups = log_step.shape[0]
    states = input_map.shape[2]
    width = input_map.shape[3]
    merged = groups * states
    channels = groups * width
    step_rate, turn_cosine, turn_sine, inject_real, inject_imaginary = factors(log_step, states)
    magnitude = jnp.exp(-0.5 * step_rate[None, :] + decay_shift)[:, :, None]
    decay_real = (magnitude * turn_cosine[None]).reshape(row_count, merged)
    decay_imaginary = (magnitude * turn_sine[None]).reshape(row_count, merged)
    identity = jnp.eye(groups, dtype=jnp.float32)
    spread_in = jnp.einsum("cgph,gk->hcgkp", input_map.astype(jnp.float32), identity)
    spread_in = spread_in.reshape(width, 2, groups, groups * states)
    spread_in = (
        jnp.transpose(spread_in, (2, 0, 1, 3)).reshape(channels, 2 * merged).astype(jnp.bfloat16)
    )
    drive = jnp.dot(mixer_input, spread_in, preferred_element_type=jnp.float32)
    drive_real = drive[:, :merged]
    drive_imaginary = drive[:, merged:]
    flat_inject_real = inject_real.reshape(1, merged)
    flat_inject_imaginary = inject_imaginary.reshape(1, merged)
    push_real = flat_inject_real * drive_real - flat_inject_imaginary * drive_imaginary
    push_imaginary = flat_inject_real * drive_imaginary + flat_inject_imaginary * drive_real
    total_real, total_imaginary, local_real, local_imaginary = lax.associative_scan(
        combine_parts, (decay_real, decay_imaginary, push_real, push_imaginary), axis=0
    )
    summary = (total_real[-1], total_imaginary[-1], local_real[-1], local_imaginary[-1])
    neutral = (
        jnp.ones_like(summary[0]),
        jnp.zeros_like(summary[0]),
        jnp.zeros_like(summary[0]),
        jnp.zeros_like(summary[0]),
    )
    incoming = carried_in(summary, "ep", combine_parts, neutral)
    carry_real = incoming[2]
    carry_imaginary = incoming[3]
    state_real = (
        local_real + total_real * carry_real[None] - total_imaginary * carry_imaginary[None]
    )
    state_imaginary = (
        local_imaginary + total_real * carry_imaginary[None] + total_imaginary * carry_real[None]
    )
    signed = jnp.stack([readout[0], -readout[1]], axis=0)
    spread_out = jnp.einsum("cghp,gk->cgpkh", signed, identity, precision=highest).reshape(
        2 * merged, channels
    )
    both_states = jnp.concatenate([state_real, state_imaginary], axis=1)
    mixed = jnp.dot(both_states, spread_out, precision=highest)
    activated = jax.nn.gelu(mixed).astype(jnp.bfloat16)
    mixer_out = jnp.dot(
        lax.all_gather(activated, "tp", axis=1, tiled=True),
        mixer_weight,
        preferred_element_type=jnp.float32,
    ).astype(jnp.bfloat16)
    token_count = expert_input.shape[0]
    features = expert_input.shape[1]
    top_count = routes.shape[1]
    experts = lax.axis_size("ep")
    capacity = 2 * token_count * top_count // experts
    values = expert_input.astype(jnp.float32)
    normed = (
        values * lax.rsqrt(jnp.mean(values * values, axis=-1, keepdims=True) + 1e-06) * norm_gain
    ).astype(jnp.bfloat16)
    flat_routes = routes.reshape(-1)
    onehot = (flat_routes[:, None] == jnp.arange(experts, dtype=jnp.int32)[None, :]).astype(
        jnp.int32
    )
    before = jnp.sum((jnp.cumsum(onehot, axis=0) - onehot) * onehot, axis=1)
    slot = flat_routes * capacity + before
    owner = jnp.arange(flat_routes.shape[0], dtype=jnp.int32) // top_count
    slot_token = jnp.full((experts * capacity,), token_count, jnp.int32).at[slot].set(owner)
    slice_width = down_weight.shape[2]
    received_rows = experts * capacity
    padded = jnp.concatenate([normed, jnp.zeros((1, features), jnp.bfloat16)], axis=0)
    outgoing = padded[slot_token].reshape(experts, capacity, features)
    arrived = lax.all_to_all(outgoing, "ep", split_axis=0, concat_axis=0, tiled=True).reshape(
        received_rows, features
    )
    gate_sum = jnp.dot(arrived, expert_switch_matrix[0], preferred_element_type=jnp.float32)
    up_sum = jnp.dot(arrived, up_weight[0], preferred_element_type=jnp.float32)
    expert_hidden = (jax.nn.silu(gate_sum) * up_sum).astype(jnp.bfloat16)
    shared_hidden = (
        jax.nn.silu(jnp.dot(normed, shared_gate, preferred_element_type=jnp.float32))
        * jnp.dot(normed, shared_up, preferred_element_type=jnp.float32)
    ).astype(jnp.bfloat16)
    rows_here = down_weight[0]
    routed_output = jnp.dot(
        lax.all_gather(expert_hidden, "tp", axis=1, tiled=True),
        rows_here,
        preferred_element_type=jnp.float32,
    )
    rows_here = shared_down
    common_contribution = jnp.dot(
        lax.all_gather(shared_hidden, "tp", axis=1, tiled=True),
        rows_here,
        preferred_element_type=jnp.float32,
    )
    returned = lax.all_to_all(
        routed_output.astype(jnp.bfloat16).reshape(experts, capacity, slice_width),
        "ep",
        split_axis=0,
        concat_axis=0,
        tiled=True,
    ).reshape(received_rows, slice_width)
    picked = returned[slot].reshape(token_count, top_count, slice_width).astype(jnp.float32)
    experts_out = (common_contribution + jnp.sum(route_weight[:, :, None] * picked, axis=1)).astype(
        jnp.bfloat16
    )
    return (mixer_out, experts_out)


def solution(mesh):
    placed = (
        P("ep", "tp"),
        P("tp"),
        P("ep", "tp"),
        P(None, "tp", None, None),
        P(None, "tp", None, None),
        P(None, "tp"),
        P("ep", None),
        P(),
        P("ep", None),
        P("ep", None),
        P("ep", None, "tp"),
        P("ep", None, "tp"),
        P("ep", None, "tp"),
        P(None, "tp"),
        P(None, "tp"),
        P(None, "tp"),
    )
    return jax.shard_map(
        shards,
        mesh=mesh,
        in_specs=placed,
        out_specs=(P("ep", "tp"), P("ep", "tp")),
        check_vma=False,
    )
```

profile of v0, /device:TPU:0, one launch (start us, length us, event | category | flops | bytes accessed | tf_op | source)
XLA Modules:
  0.0 417.1 jit_solution(5019103018947670209)
XLA Ops:
  15.0 3.3 gather_fusion
  18.3 6.5 %all-to-all-start = ((bf16[8,64,2048]{2,1,0:T(8,128)(2,1)}), bf16[8,64,2048]{2,1,0:T(8,128)(2,1)}, u32[]{:S(2)}, u32[]{:S(2)}) async-start(bf16[8,64,2048]{2,1,0:T(8,128)(2,1)} %bitcast.95), calls=%async_computation | async-start | bytes 4194304 | tf_op jit(solution)/shard_map/all_to_all | solution.py:144
  30.9 2.3 copy.44
  42.6 3.3 slice.500
  45.8 3.3 slice.506
  49.1 3.2 slice.502
  52.4 3.2 slice.507
  55.6 4.1 multiply_subtract_fusion.3
  73.3 2.5 add_add_fusion.4
  180.5 3.3 slice.499
  183.8 3.3 slice.609
  221.4 2.7 pad.260
  226.8 2.8 subtract_add_fusion.1
  230.6 14.6 %all-gather.3 = f32[8,1,1024]{2,1,0:T(1,128)S(1)} all-gather(f32[1,1,1024]{2,1,0:T(1,128)S(1)} %add_bitcast_fusion), channel_id=1, replica_groups=mesh['ep'=8,'tp'=4] {'ep'}, dimensions={0}, use_global_device_ids=true | all-gather | bytes 36864 | tf_op jit(solution)/shard_map/all_gather | solution.py:9
  248.0 2.3 pad_maximum_fusion
  250.3 4.7 %pad.225 = f32[256,1024]{1,0:T(8,128)} pad(f32[128,1024]{1,0:T(8,128)} %pad_maximum_fusion, f32[]{:T(128)} %constant.73.clone.1), padding=0_1_1x0_0_0 | pad | bytes 1572868 | tf_op jit(solution)/shard_map/pad | solution.py:92
  255.8 14.1 %all-gather.2 = f32[8,1,1024]{2,1,0:T(1,128)S(1)} all-gather(f32[1,1,1024]{2,1,0:T(1,128)S(1)} %add_bitcast_fusion.1), channel_id=1, replica_groups=mesh['ep'=8,'tp'=4] {'ep'}, dimensions={0}, use_global_device_ids=true | all-gather | bytes 36864 | tf_op jit(solution)/shard_map/all_gather | solution.py:9
  279.0 5.3 %fusion.4 = f32[512,1024]{1,0:T(8,128)S(1)} fusion(bf16[512,2048]{1,0:T(8,128)(2,1)} %bitcast.20, bf16[1,2048,1024]{2,1,0:T(8,128)(2,1)} %param.28), kind=kOutput, calls=%fused_computation.13 | convolution fusion | flops 2147483648 | bytes 8388608 | tf_op jit(solution)/shard_map/dot_general | solution.py:147
  284.4 5.1 %multiply_convert_fusion.1 = bf16[512,1024]{1,0:T(8,128)(2,1)} fusion(f32[512,1024]{1,0:T(8,128)S(1)} %fusion.4, bf16[512,2048]{1,0:T(8,128)(2,1)} %bitcast.20, bf16[1,2048,1024]{2,1,0:T(8,128)(2,1)S(1)} %copy-done.62), kind=kOutput, calls=%fused_computation.23 | convolution fusion | flops 2150629376 | bytes 9437184 | tf_op jit(solution)/shard_map/dot_general | solution.py:148
  294.9 2.7 pad.258
  304.1 2.3 multiply_add_fusion.2
  307.5 14.1 %all-gather.1 = f32[8,1,1024]{2,1,0:T(1,128)S(1)} all-gather(f32[1,1,1024]{2,1,0:T(1,128)S(1)} %add_bitcast_fusion.2), channel_id=1, replica_groups=mesh['ep'=8,'tp'=4] {'ep'}, dimensions={0}, use_global_device_ids=true | all-gather | bytes 36864 | tf_op jit(solution)/shard_map/all_gather | solution.py:9
  324.7 4.6 %pad.256 = f32[256,1024]{1,0:T(8,128)} pad(f32[128,1024]{1,0:T(8,128)} %add.626, f32[]{:T(128)} %constant.73.clone.1), padding=1_0_1x0_0_0 | pad | bytes 1572868 | tf_op jit(solution)/shard_map/pad | solution.py:92
  330.1 14.1 %all-gather = f32[8,1,1024]{2,1,0:T(1,128)S(1)} all-gather(f32[1,1,1024]{2,1,0:T(1,128)S(1)} %add_bitcast_fusion.3), channel_id=1, replica_groups=mesh['ep'=8,'tp'=4] {'ep'}, dimensions={0}, use_global_device_ids=true | all-gather | bytes 36864 | tf_op jit(solution)/shard_map/all_gather | solution.py:9
  345.9 2.6 multiply_bitcast_fusion
  348.6 5.6 %multiply_subtract_fusion = (f32[256,1024]{1,0:T(8,128)}, f32[256,1024]{1,0:T(8,128)}) fusion(f32[256,1024]{1,0:T(8,128)} %pad.225, f32[256,1024]{1,0:T(8,128)} %copy-done.7, f32[1024]{0:T(1024)S(1)} %get-tuple-element.73, f32[1024]{0:T(1024)S(1)} %get-tuple-element.72, f32[256,1024]{1,0:T(8,128)} %copy-done.8, f32[256,1024]{1,0:T(8,128)} %pad.258, ...), kind=kLoop, calls=%fused_computation.36 | loop fusion | flops 3145728 | bytes 10493952 | tf_op jit(solution)/shard_map/sub | solution.py:106
  354.1 6.6 %fusion.13 = bf16[512,512]{1,0:T(8,128)(2,1)} fusion(bf16[512,4096]{1,0:T(8,128)(2,1)} %all-gather.6.cloned.1.call-done, bf16[1,4096,512]{2,1,0:T(8,128)(2,1)} %param.30), kind=kOutput, calls=%fused_computation.26 | convolution fusion | flops 2147745792 | bytes 8912896 | tf_op jit(solution)/shard_map/dot_general | solution.py:155
  360.7 10.6 %all-to-all-start.1 = ((bf16[8,64,512]{2,1,0:T(8,128)(2,1)}), bf16[8,64,512]{2,1,0:T(8,128)(2,1)S(1)}, u32[]{:S(2)}, u32[]{:S(2)}) async-start(bf16[8,64,512]{2,1,0:T(8,128)(2,1)} %bitcast.24), calls=%async_computation.1 | async-start | bytes 1048576 | tf_op jit(solution)/shard_map/all_to_all | solution.py:166
  372.9 5.1 %reshape.245 = f32[2048,256]{0,1:T(8,128)} reshape(f32[2,16,64,16,16]{2,1,0,4,3:T(8,128)} %multiply_bitcast_fusion) | data formatting | bytes 4194304 | tf_op jit(solution)/shard_map/reshape | solution.py:112
  378.1 10.6 %all_gather.26 = bf16[128,1024]{1,0:T(8,128)(2,1)S(1)} all-gather(bf16[128,256]{1,0:T(8,128)(2,1)S(1)} %fusion.17), channel_id=1, replica_groups=mesh['ep'=8,'tp'=4] {'tp'}, dimensions={1}, use_global_device_ids=true | all-gather | bytes 327680 | tf_op jit(solution)/shard_map/all_gather | solution.py:162
  388.7 3.8 fusion.30
  392.5 12.1 %all_gather.25 = bf16[256,1024]{1,0:T(8,128)(2,1)S(1)} all-gather(bf16[256,256]{1,0:T(8,128)(2,1)S(1)} %fusion.30), channel_id=1, replica_groups=mesh['ep'=8,'tp'=4] {'tp'}, dimensions={1}, use_global_device_ids=true | all-gather | bytes 655360 | tf_op jit(solution)/shard_map/all_gather | solution.py:119
  (430 shorter events, 216.7 us)
Async XLA Ops:
  7.2 397.5 %copy-start = (bf16[1024,512]{1,0:T(8,128)(2,1)S(1)}, bf16[1024,512]{1,0:T(8,128)(2,1)}, u32[]{:S(2)}) copy-start(bf16[1024,512]{1,0:T(8,128)(2,1)} %param.23) | copy-start | bytes 3145732
  18.3 6.8 %copy-start.61 = (f32[16]{0:T(128)S(1)}, f32[16]{0:T(128)}, u32[]{:S(2)}) copy-start(f32[16]{0:T(128)} %param.19) | copy-start | bytes 196
  18.3 7.4 %copy-start.55 = (f32[256,16]{0,1:T(8,128)S(1)}, f32[256,16]{0,1:T(8,128)}, u32[]{:S(2)}) copy-start(f32[256,16]{0,1:T(8,128)} %param.20) | copy-start | bytes 49156
  18.3 260.7 %all-to-all-start = ((bf16[8,64,2048]{2,1,0:T(8,128)(2,1)}), bf16[8,64,2048]{2,1,0:T(8,128)(2,1)}, u32[]{:S(2)}, u32[]{:S(2)}) async-start(bf16[8,64,2048]{2,1,0:T(8,128)(2,1)} %bitcast.95), calls=%async_computation | async-start | bytes 4194304 | tf_op jit(solution)/shard_map/all_to_all | solution.py:144
  24.8 329.4 %all-gather.6.cloned.1.call-start = ((), (), s32[]{:S(2)}) async-start(), calls=%async_computation.2 | async-start | bytes 5242880 | tf_op jit(solution)/shard_map/all_gather | solution.py:156
  75.8 87.9 %copy-start.15 = (f32[64,1024]{1,0:T(8,128)}, f32[64,1024]{1,0:T(8,128)S(1)}, u32[]{:S(2)}) copy-start(f32[64,1024]{1,0:T(8,128)S(1)} %get-tuple-element.131) | copy-start | bytes 786436
  127.1 12.7 %copy-start.34 = (f32[4,1024]{1,0:T(4,128)}, f32[4,1024]{1,0:T(4,128)S(1)}, u32[]{:S(2)}) copy-start(f32[4,1024]{1,0:T(4,128)S(1)} %get-tuple-element.174) | copy-start | bytes 49156
  190.7 25.6 %copy-start.21 = (f32[15,1024]{1,0:T(8,128)S(1)}, f32[15,1024]{1,0:T(8,128)}, u32[]{:S(2)}) copy-start(f32[15,1024]{1,0:T(8,128)} %slice.528) | copy-start | bytes 184324
  190.7 25.6 %copy-start.23 = (f32[15,1024]{1,0:T(8,128)S(1)}, f32[15,1024]{1,0:T(8,128)}, u32[]{:S(2)}) copy-start(f32[15,1024]{1,0:T(8,128)} %slice.591) | copy-start | bytes 184324
  190.8 25.6 %copy-start.29 = (f32[15,1024]{1,0:T(8,128)S(1)}, f32[15,1024]{1,0:T(8,128)}, u32[]{:S(2)}) copy-start(f32[15,1024]{1,0:T(8,128)} %slice.595) | copy-start | bytes 184324
  190.8 25.7 %copy-start.30 = (f32[15,1024]{1,0:T(8,128)S(1)}, f32[15,1024]{1,0:T(8,128)}, u32[]{:S(2)}) copy-start(f32[15,1024]{1,0:T(8,128)} %slice.599) | copy-start | bytes 184324
  190.8 25.7 %copy-start.54 = (f32[1,1024]{1,0:T(1,128)S(1)}, f32[1,1024]{1,0:T(1,128)}, u32[]{:S(2)}) copy-start(f32[1,1024]{1,0:T(1,128)} %slice.700) | copy-start | bytes 12292
  190.8 25.8 %copy-start.53 = (f32[1,1024]{1,0:T(1,128)S(1)}, f32[1,1024]{1,0:T(1,128)}, u32[]{:S(2)}) copy-start(f32[1,1024]{1,0:T(1,128)} %slice.665) | copy-start | bytes 12292
  229.8 25.2 %copy-start.6 = (f32[256,1024]{1,0:T(8,128)}, f32[256,1024]{1,0:T(8,128)S(1)}, u32[]{:S(2)}) copy-start(f32[256,1024]{1,0:T(8,128)S(1)} %pad.259) | copy-start | bytes 3145732
  248.0 36.4 %copy-start.7 = (f32[256,1024]{1,0:T(8,128)}, f32[256,1024]{1,0:T(8,128)S(1)}, u32[]{:S(2)}) copy-start(f32[256,1024]{1,0:T(8,128)S(1)} %pad.226) | copy-start | bytes 3145732
  279.0 5.3 %copy-start.62 = (bf16[1,2048,1024]{2,1,0:T(8,128)(2,1)S(1)}, bf16[1,2048,1024]{2,1,0:T(8,128)(2,1)}, u32[]{:S(2)}) copy-start(bf16[1,2048,1024]{2,1,0:T(8,128)(2,1)} %param.29) | copy-start | bytes 12582916
  284.4 5.3 %copy-start.27 = (f32[7,1024]{1,0:T(8,128)S(1)}, f32[7,1024]{1,0:T(8,128)}, u32[]{:S(2)}) copy-start(f32[7,1024]{1,0:T(8,128)} %slice.538) | copy-start | bytes 86020
  284.4 5.3 %copy-start.28 = (f32[7,1024]{1,0:T(8,128)S(1)}, f32[7,1024]{1,0:T(8,128)}, u32[]{:S(2)}) copy-start(f32[7,1024]{1,0:T(8,128)} %slice.585) | copy-start | bytes 86020
  284.4 5.3 %copy-start.51 = (f32[1,1024]{1,0:T(1,128)S(1)}, f32[1,1024]{1,0:T(1,128)}, u32[]{:S(2)}) copy-start(f32[1,1024]{1,0:T(1,128)} %slice.738) | copy-start | bytes 12292
  284.4 5.4 %copy-start.50 = (f32[1,1024]{1,0:T(1,128)S(1)}, f32[1,1024]{1,0:T(1,128)}, u32[]{:S(2)}) copy-start(f32[1,1024]{1,0:T(1,128)} %slice.717) | copy-start | bytes 12292
  297.6 6.5 %copy-start.3 = (f32[127,1024]{1,0:T(8,128)S(1)}, f32[127,1024]{1,0:T(8,128)}, u32[]{:S(2)}) copy-start(f32[127,1024]{1,0:T(8,128)} %slice.499) | copy-start | bytes 1560580
  297.6 6.5 %copy-start.4 = (f32[127,1024]{1,0:T(8,128)S(1)}, f32[127,1024]{1,0:T(8,128)}, u32[]{:S(2)}) copy-start(f32[127,1024]{1,0:T(8,128)} %slice.609) | copy-start | bytes 1560580
  306.5 15.1 %copy-start.40 = (f32[16,64]{1,0:T(8,128)S(1)}, f32[16,64]{1,0:T(8,128)}, u32[]{:S(2)}) copy-start(f32[16,64]{1,0:T(8,128)} %get-tuple-element.75) | copy-start | bytes 12292
  306.5 15.2 %copy-start.14 = (f32[127,1024]{1,0:T(8,128)S(1)}, f32[127,1024]{1,0:T(8,128)}, u32[]{:S(2)}) copy-start(f32[127,1024]{1,0:T(8,128)} %get-tuple-element.103) | copy-start | bytes 1560580
  306.7 15.0 %copy-start.8 = (f32[256,1024]{1,0:T(8,128)}, f32[256,1024]{1,0:T(8,128)S(1)}, u32[]{:S(2)}) copy-start(f32[256,1024]{1,0:T(8,128)S(1)} %pad.257) | copy-start | bytes 3145732
  321.7 22.5 %copy-start.31 = (f32[2,16,16,64]{3,2,1,0:T(8,128)S(1)}, f32[2,16,16,64]{3,2,1,0:T(8,128)}, u32[]{:S(2)}) copy-start(f32[2,16,16,64]{3,2,1,0:T(8,128)} %param.22) | copy-start | bytes 393220
  322.6 21.8 %copy-start.2 = (bf16[128,2048]{1,0:T(8,128)(2,1)S(1)}, bf16[128,2048]{1,0:T(8,128)(2,1)}, u32[]{:S(2)}) copy-start(bf16[128,2048]{1,0:T(8,128)(2,1)} %copy-done.1) | copy-start | bytes 1572868
  324.7 19.6 %copy-start.9 = (f32[256,1024]{1,0:T(8,128)}, f32[256,1024]{1,0:T(8,128)S(1)}, u32[]{:S(2)}) copy-start(f32[256,1024]{1,0:T(8,128)S(1)} %pad.255) | copy-start | bytes 3145732
  324.7 21.2 %copy-start.37 = (f32[16,16]{0,1:T(8,128)S(1)}, f32[16,16]{0,1:T(8,128)}, u32[]{:S(2)}) copy-start(f32[16,16]{0,1:T(8,128)} %copy-done.36) | copy-start | bytes 3076
  360.7 45.1 %all-to-all-start.1 = ((bf16[8,64,512]{2,1,0:T(8,128)(2,1)}), bf16[8,64,512]{2,1,0:T(8,128)(2,1)S(1)}, u32[]{:S(2)}, u32[]{:S(2)}) async-start(bf16[8,64,512]{2,1,0:T(8,128)(2,1)} %bitcast.24), calls=%async_computation.1 | async-start | bytes 1048576 | tf_op jit(solution)/shard_map/all_to_all | solution.py:166
  372.9 15.8 %copy-start.11 = (f32[256,1024]{1,0:T(8,128)S(1)}, f32[256,1024]{1,0:T(8,128)}, u32[]{:S(2)}) copy-start(f32[256,1024]{1,0:T(8,128)} %get-tuple-element.98) | copy-start | bytes 3145732
  388.7 16.0 %copy-start.58 = (s32[256,1]{0,1:T(1,128)S(1)}, s32[256,1]{0,1:T(1,128)}, u32[]{:S(2)}) copy-start(s32[256,1]{0,1:T(1,128)} %copy-done.57) | copy-start | bytes 3076
  (34 other events, 82.4 us)
Sparse Core Ops, SparseCore 0:
  289.7 53.4 all-gather.5
where the time goes:
time: 424 us; the launch traced here: 417 us
  local copies, waits for them, and re-layouts  208 us (49%)
  blocking collectives  79.7 us (19%)
  other arithmetic  68.9 us (16%)
  matrix products  27.7 us (7%)
  starting transfers between devices  17.3 us (4%)
  between operations  15.6 us (4%)
    slice x108, local copies, waits for them, and re-layouts, shards(): lax.associative_scan(combine_parts, (decay_real, decay_imaginary, push_re...  155 us
    all_gather x4, blocking collectives, carried_in(): gathered = jax.tree.map(lambda a: lax.all_gather(a, axis), part)  56.9 us
    pad x56, local copies, waits for them, and re-layouts, shards(): lax.associative_scan(combine_parts, (decay_real, decay_imaginary, push_re...  28.3 us
    concatenate x28, other arithmetic, shards(): lax.associative_scan(combine_parts, (decay_real, decay_imaginary, push_re...  13 us
    all_gather x1, blocking collectives, shards(): lax.all_gather(activated, 'tp', axis=1, tiled=True)  12.1 us
    all_gather x1, blocking collectives, shards(): lax.all_gather(shared_hidden, 'tp', axis=1, tiled=True)  10.6 us
    all_to_all x1, starting transfers between devices, shards(): lax.all_to_all(routed_output.astype(jnp.bfloat16).reshape(experts, capaci...  10.6 us
    add x9, other arithmetic, combine_parts(): late_real * early_shift_imaginary + late_imaginary * early_shift_real  9.13 us
  transfers between devices with their start and end apart: 3, of which 0 were waited for; matrix products, arithmetic and copies ran while one was open for 65% of the time, Pallas kernels for 0%

commit v1 on v0

v1 whole, which is shorter than its diff:
```python
import functools

import jax
import jax.numpy as jnp
from jax import lax
from jax.experimental import pallas as pl
from jax.experimental.pallas import tpu as pltpu
from jax.sharding import PartitionSpec as P

MESH = pl.DeviceIdType.MESH
SUBLANES = 8
NT = (((1,), (1,)), ((), ()))


def factors(log_step, states):
    step_rate = jnp.exp(log_step)
    frequency = jnp.pi * jnp.arange(states, dtype=jnp.float32)
    angle = step_rate[:, None] * frequency[None, :]
    turn_cosine = jnp.cos(angle)
    turn_sine = jnp.sin(angle)
    base = jnp.exp(-0.5 * step_rate)[:, None]
    base_real = base * turn_cosine
    starting_quadrature = base * turn_sine
    inverse = 1.0 / (0.25 + frequency * frequency)[None, :]
    lowered = base_real - 1.0
    inject_real = (-0.5 * lowered + starting_quadrature * frequency[None, :]) * inverse
    inject_imaginary = (-0.5 * starting_quadrature - lowered * frequency[None, :]) * inverse
    return (step_rate, turn_cosine, turn_sine, inject_real, inject_imaginary)


def times(ar, ai, br, bi):
    return ar * br - ai * bi, ar * bi + ai * br


def iota(shape, dim):
    return lax.broadcasted_iota(jnp.int32, shape, dim)


def spread(shape, period):
    return (iota(shape, 1) % period == iota(shape, 0)).astype(jnp.bfloat16)


def halves(a):
    high = a.astype(jnp.bfloat16)
    return high, (a - high.astype(jnp.float32)).astype(jnp.bfloat16)


def dot(a, b, dims=None):
    if dims is None:
        return jnp.dot(a, b, preferred_element_type=jnp.float32)
    return lax.dot_general(a, b, dims, preferred_element_type=jnp.float32)


def drive_into(x_ref, rate_ref, shift_ref, map_ref, table_ref, mag, push_re, push_im, states):
    rows, channels = x_ref.shape
    merged = mag.shape[1]
    groups = shift_ref.shape[1]
    width = channels // groups
    steps = rows // SUBLANES
    place = iota((rows, rows), 0)
    order = (iota((rows, rows), 1) == (place % SUBLANES) * steps + place // SUBLANES).astype(
        jnp.bfloat16
    )
    level = jnp.exp(-0.5 * jnp.exp(rate_ref[...]) + shift_ref[...])
    high, rest = halves(level)
    middle = rest
    low = ((level - high.astype(jnp.float32)) - middle.astype(jnp.float32)).astype(jnp.bfloat16)
    widen = (iota((groups, merged), 1) // states == iota((groups, merged), 0)).astype(jnp.bfloat16)
    total = None
    for piece in (high, middle, low):
        part = dot(dot(order, piece).astype(jnp.bfloat16), widen)
        total = part if total is None else total + part
    mag[...] = total
    x = dot(order, x_ref[...]).astype(jnp.bfloat16)
    repeat = spread((width, channels), width)
    mine = iota((merged, channels), 0) // states == iota((merged, channels), 1) // width
    drives = []
    for c in range(2):
        wide = jnp.where(mine, dot(map_ref[c], repeat), 0.0).astype(jnp.bfloat16)
        drives.append(dot(x, wide, NT))
    re, im = times(table_ref[2:3, :], table_ref[3:4, :], drives[0], drives[1])
    push_re[...] = re
    push_im[...] = im


def sweep(table_ref, mag, push_re, push_im, start_re, start_im, keep):
    rows, merged = mag.shape
    turn_re = jnp.broadcast_to(table_ref[0:1, :], (SUBLANES, merged))
    turn_im = jnp.broadcast_to(table_ref[1:2, :], (SUBLANES, merged))

    def one(j, carry):
        re, im, product = carry
        at = pl.ds(pl.multiple_of(j * SUBLANES, SUBLANES), SUBLANES)
        level = mag[at, :]
        next_re, next_im = times(turn_re, turn_im, re, im)
        next_re = level * next_re + push_re[at, :]
        next_im = level * next_im + push_im[at, :]
        if keep:
            push_re[at, :] = next_re
            push_im[at, :] = next_im
        else:
            product = product * level
        return next_re, next_im, product

    product = jnp.ones((SUBLANES, merged), jnp.float32)
    if keep:
        def pair(j, carry):
            return one(j, carry + (None,))[:2]
        return lax.fori_loop(0, rows // SUBLANES, pair, (start_re, start_im))
    return lax.fori_loop(0, rows // SUBLANES, one, (start_re, start_im, product))


def join(table_ref, ends_re, ends_im, product, pre, steps):
    merged = ends_re.shape[1]
    wr, wi = table_ref[0:1, :], table_ref[1:2, :]
    power = 1
    while power < steps:
        wr, wi = times(wr, wi, wr, wi)
        power *= 2
    cr = jnp.zeros((1, merged), jnp.float32)
    ci = cr
    ar = cr + 1.0
    ai = cr
    for s in range(SUBLANES):
        for i, v in enumerate((cr, ci, ar, ai)):
            pre[i, s : s + 1, :] = v
        level = product[s : s + 1]
        fr, fi = level * wr, level * wi
        tr, ti = times(fr, fi, cr, ci)
        cr, ci = tr + ends_re[s : s + 1], ti + ends_im[s : s + 1]
        ar, ai = times(fr, fi, ar, ai)
    return cr, ci, ar, ai


def read_states(readout_ref, push_re, push_im, states):
    rows, merged = push_re.shape
    channels = readout_ref.shape[1]
    width = channels * states // merged
    repeat = spread((states, merged), states)
    mine = iota((channels, merged), 1) // states == iota((channels, merged), 0) // width
    total = None
    for c, ref in enumerate((push_re, push_im)):
        high, low = halves(ref[...])
        back = readout_ref[c] if c == 0 else -readout_ref[c]
        wide_high, wide_low = (
            jnp.where(mine, dot(half, repeat), 0.0).astype(jnp.bfloat16) for half in halves(back)
        )
        part = dot(high, wide_high, NT) + (dot(low, wide_high, NT) + dot(high, wide_low, NT))
        total = part if total is None else total + part
    place = iota((rows, rows), 0)
    steps = rows // SUBLANES
    order = (iota((rows, rows), 1) == (place % steps) * SUBLANES + place // steps).astype(
        jnp.bfloat16
    )
    cube = total + 0.044715 * (total * total * total)
    active = (0.5 * total * (1.0 + jnp.tanh(0.7978845608028654 * cube))).astype(jnp.bfloat16)
    return dot(order, active).astype(jnp.bfloat16)


def mixer_kernel(
    n_ep, n_tp, states,
    x_ref, rate_ref, shift_ref, map_ref, readout_ref, table_ref, weight_ref,
    out_ref,
    mag, push_re, push_im, pre, summary, active,
    ep_send, ep_recv, tp_send, tp_recv,
):
    ep = lax.axis_index("ep")
    tp = lax.axis_index("tp")
    rows, channels = x_ref.shape
    merged = mag.shape[1]
    barrier = pltpu.get_barrier_semaphore()
    for d in range(1, n_ep):
        pl.semaphore_signal(
            barrier, inc=1, device_id={"ep": lax.rem(ep + d, n_ep)}, device_id_type=MESH
        )
    for d in range(1, n_tp):
        pl.semaphore_signal(
            barrier, inc=1, device_id={"tp": lax.rem(tp + d, n_tp)}, device_id_type=MESH
        )
    drive_into(x_ref, rate_ref, shift_ref, map_ref, table_ref, mag, push_re, push_im, states)
    zero = jnp.zeros((SUBLANES, merged), jnp.float32)
    ends_re, ends_im, product = sweep(table_ref, mag, push_re, push_im, zero, zero, False)
    end = join(table_ref, ends_re, ends_im, product, pre, rows // SUBLANES)
    for i, v in enumerate(end):
        summary[ep, i : i + 1, :] = v
    pl.semaphore_wait(barrier, n_ep + n_tp - 2)
    copies = []
    for d in range(1, n_ep):
        copy = pltpu.make_async_remote_copy(
            src_ref=summary.at[ep],
            dst_ref=summary.at[ep],
            send_sem=ep_send.at[d],
            recv_sem=ep_recv.at[d],
            device_id={"ep": lax.rem(ep + d, n_ep)},
            device_id_type=MESH,
        )
        copy.start()
        copies.append(copy)
    for copy in copies:
        copy.wait()

    def fold(e, carry):
        part = summary[e]
        re, im = times(part[2:3], part[3:4], carry[0], carry[1])
        return re + part[0:1], im + part[1:2]

    nothing = jnp.zeros((1, merged), jnp.float32)
    in_re, in_im = lax.fori_loop(0, ep, fold, (nothing, nothing))
    add_re, add_im = times(pre[2], pre[3], in_re, in_im)
    sweep(table_ref, mag, push_re, push_im, pre[0] + add_re, pre[1] + add_im, True)
    active[tp] = read_states(readout_ref, push_re, push_im, states)
    copies = []
    for d in range(1, n_tp):
        copy = pltpu.make_async_remote_copy(
            src_ref=active.at[tp],
            dst_ref=active.at[tp],
            send_sem=tp_send.at[d],
            recv_sem=tp_recv.at[d],
            device_id={"tp": lax.rem(tp + d, n_tp)},
            device_id_type=MESH,
        )
        copy.start()
        copies.append(copy)
    total = None
    for d in range(n_tp):
        if d > 0:
            copies[d - 1].wait()
        owner = lax.rem(tp + n_tp - d, n_tp)
        at = pl.ds(pl.multiple_of(owner * channels, channels), channels)
        part = dot(active[owner], weight_ref[at, :])
        total = part if total is None else total + part
    out_ref[...] = total.astype(out_ref.dtype)


def mixer(mixer_input, log_step, decay_shift, input_map, readout, mixer_weight):
    n_ep, n_tp = lax.axis_size("ep"), lax.axis_size("tp")
    rows, channels = mixer_input.shape
    groups = log_step.shape[0]
    states, width = input_map.shape[2:]
    merged = groups * states
    _, cosine, sine, inject_re, inject_im = factors(log_step, states)
    table = jnp.stack([a.reshape(merged) for a in (cosine, sine, inject_re, inject_im)])
    f32 = jnp.float32
    return pl.pallas_call(
        functools.partial(mixer_kernel, n_ep, n_tp, states),
        out_shape=jax.ShapeDtypeStruct((rows, mixer_weight.shape[1]), jnp.bfloat16),
        in_specs=[pl.BlockSpec(memory_space=pltpu.VMEM)] * 7,
        out_specs=pl.BlockSpec(memory_space=pltpu.VMEM),
        scratch_shapes=[
            pltpu.VMEM((rows, merged), f32),
            pltpu.VMEM((rows, merged), f32),
            pltpu.VMEM((rows, merged), f32),
            pltpu.VMEM((4, SUBLANES, merged), f32),
            pltpu.VMEM((n_ep, 4, merged), f32),
            pltpu.VMEM((n_tp, rows, channels), jnp.bfloat16),
            pltpu.SemaphoreType.DMA((n_ep,)),
            pltpu.SemaphoreType.DMA((n_ep,)),
            pltpu.SemaphoreType.DMA((n_tp,)),
            pltpu.SemaphoreType.DMA((n_tp,)),
        ],
        compiler_params=pltpu.CompilerParams(
            collective_id=0, has_side_effects=True, vmem_limit_bytes=40 * 1024 * 1024
        ),
        cost_estimate=pl.CostEstimate(
            flops=20_000_000_000, bytes_accessed=10_000_000, transcendentals=0
        ),
        name="mixer",
    )(
        mixer_input,
        log_step.reshape(1, groups),
        decay_shift,
        input_map.reshape(2, merged, width),
        readout.reshape(2, channels, states),
        table,
        mixer_weight,
    )


def shards(
    mixer_input,
    log_step,
    decay_shift,
    input_map,
    readout,
    mixer_weight,
    expert_input,
    norm_gain,
    routes,
    route_weight,
    expert_switch_matrix,
    up_weight,
    down_weight,
    shared_gate,
    shared_up,
    shared_down,
):
    mixer_out = mixer(mixer_input, log_step, decay_shift, input_map, readout, mixer_weight)
    token_count = expert_input.shape[0]
    features = expert_input.shape[1]
    top_count = routes.shape[1]
    experts = lax.axis_size("ep")
    capacity = 2 * token_count * top_count // experts
    values = expert_input.astype(jnp.float32)
    normed = (
        values * lax.rsqrt(jnp.mean(values * values, axis=-1, keepdims=True) + 1e-06) * norm_gain
    ).astype(jnp.bfloat16)
    flat_routes = routes.reshape(-1)
    onehot = (flat_routes[:, None] == jnp.arange(experts, dtype=jnp.int32)[None, :]).astype(
        jnp.int32
    )
    before = jnp.sum((jnp.cumsum(onehot, axis=0) - onehot) * onehot, axis=1)
    slot = flat_routes * capacity + before
    owner = jnp.arange(flat_routes.shape[0], dtype=jnp.int32) // top_count
    slot_token = jnp.full((experts * capacity,), token_count, jnp.int32).at[slot].set(owner)
    slice_width = down_weight.shape[2]
    received_rows = experts * capacity
    padded = jnp.concatenate([normed, jnp.zeros((1, features), jnp.bfloat16)], axis=0)
    outgoing = padded[slot_token].reshape(experts, capacity, features)
    arrived = lax.all_to_all(outgoing, "ep", split_axis=0, concat_axis=0, tiled=True).reshape(
        received_rows, features
    )
    gate_sum = jnp.dot(arrived, expert_switch_matrix[0], preferred_element_type=jnp.float32)
    up_sum = jnp.dot(arrived, up_weight[0], preferred_element_type=jnp.float32)
    expert_hidden = (jax.nn.silu(gate_sum) * up_sum).astype(jnp.bfloat16)
    shared_hidden = (
        jax.nn.silu(jnp.dot(normed, shared_gate, preferred_element_type=jnp.float32))
        * jnp.dot(normed, shared_up, preferred_element_type=jnp.float32)
    ).astype(jnp.bfloat16)
    rows_here = down_weight[0]
    routed_output = jnp.dot(
        lax.all_gather(expert_hidden, "tp", axis=1, tiled=True),
        rows_here,
        preferred_element_type=jnp.float32,
    )
    rows_here = shared_down
    common_contribution = jnp.dot(
        lax.all_gather(shared_hidden, "tp", axis=1, tiled=True),
        rows_here,
        preferred_element_type=jnp.float32,
    )
    returned = lax.all_to_all(
        routed_output.astype(jnp.bfloat16).reshape(experts, capacity, slice_width),
        "ep",
        split_axis=0,
        concat_axis=0,
        tiled=True,
    ).reshape(received_rows, slice_width)
    picked = returned[slot].reshape(token_count, top_count, slice_width).astype(jnp.float32)
    experts_out = (common_contribution + jnp.sum(route_weight[:, :, None] * picked, axis=1)).astype(
        jnp.bfloat16
    )
    return (mixer_out, experts_out)


def solution(mesh):
    placed = (
        P("ep", "tp"),
        P("tp"),
        P("ep", "tp"),
        P(None, "tp", None, None),
        P(None, "tp", None, None),
        P(None, "tp"),
        P("ep", None),
        P(),
        P("ep", None),
        P("ep", None),
        P("ep", None, "tp"),
        P("ep", None, "tp"),
        P("ep", None, "tp"),
        P(None, "tp"),
        P(None, "tp"),
        P(None, "tp"),
    )
    return jax.shard_map(
        shards,
        mesh=mesh,
        in_specs=placed,
        out_specs=(P("ep", "tp"), P("ep", "tp")),
        check_vma=False,
    )
```

time: 424 us -> 198 us (0.47); the launches traced: 417 us -> 197 us
  local copies, waits for them, and re-layouts: 208 us -> 11.6 us
  other arithmetic: 68.9 us -> 4.79 us
  waiting for transfers between devices: 0.02 us -> 50.5 us
  Pallas kernels: 0 us -> 29.3 us
  blocking collectives: 79.7 us -> 65.5 us
  starting transfers between devices: 17.3 us -> 4.64 us
  matrix products: 27.7 us -> 16.8 us
    slice x109 -> x1, local copies, waits for them, and re-layouts: 155 us -> 0.21 us  [the longest x108 155 us: shards(): lax.associative_scan(combine_parts, (decay_real, decay_imaginary, push_re...]
    all_gather x5 -> x0, blocking collectives: 69 us -> none  [the longest x4 56.9 us: carried_in(): gathered = jax.tree.map(lambda a: lax.all_gather(a, axis), part)]
    all_to_all x0 -> x1, blocking collectives: none -> 55.6 us  [shards(): lax.all_to_all(outgoing, 'ep', split_axis=0, concat_axis=0, tiled=True)]
    all_gather x1, waiting for transfers between devices: 0.01 us -> 50.5 us  [shards(): lax.all_gather(expert_hidden, 'tp', axis=1, tiled=True)]
    pallas_call x0 -> x1, Pallas kernels: none -> 29.3 us  [mixer(): pl.pallas_call(functools.partial(mixer_kernel, n_ep, n_tp, states), out_s...]
    pad x56 -> x0, local copies, waits for them, and re-layouts: 28.3 us -> none  [shards(): lax.associative_scan(combine_parts, (decay_real, decay_imaginary, push_re...]
    add x47 -> x0, other arithmetic: 27 us -> none  [the longest x9 9.13 us: combine_parts(): late_real * early_shift_imaginary + late_imaginary * early_shift_real]
    sub x5 -> x0, other arithmetic: 15.1 us -> none  [the longest x3 7.67 us: combine_parts(): joint_real = late_real * early_real - late_imaginary * early_imaginary]
  transfers between devices with their start and end apart: 3 -> 2, of which waited for: 0 -> 1; matrix products, arithmetic and copies ran while one was open for 65% -> 2% of each run, Pallas kernels for 0% -> 15%
where the time goes in v1:
time: 198 us; the launch traced here: 197 us
  blocking collectives  65.5 us (33%)
  waiting for transfers between devices  50.5 us (26%)
  Pallas kernels  29.3 us (15%)
  matrix products  16.8 us (8%)
  between operations  14.3 us (7%)
  local copies, waits for them, and re-layouts  11.6 us (6%)
  other arithmetic  4.79 us (2%)
  starting transfers between devices  4.64 us (2%)
    all_to_all x1, blocking collectives, shards(): lax.all_to_all(outgoing, 'ep', split_axis=0, concat_axis=0, tiled=True)  55.6 us
    all_gather x1, waiting for transfers between devices, shards(): lax.all_gather(expert_hidden, 'tp', axis=1, tiled=True)  50.5 us
    pallas_call x1, Pallas kernels, mixer(): pl.pallas_call(functools.partial(mixer_kernel, n_ep, n_tp, states), out_s...  29.3 us
    all_gather x1, blocking collectives, shards(): lax.all_gather(shared_hidden, 'tp', axis=1, tiled=True)  9.81 us
    dot_general x1, matrix products, shards(): jnp.dot(lax.all_gather(expert_hidden, 'tp', axis=1, tiled=True), rows_her...  6.58 us
    all_to_all x1, starting transfers between devices, shards(): lax.all_to_all(routed_output.astype(jnp.bfloat16).reshape(experts, capaci...  4.61 us
  transfers between devices with their start and end apart: 2, of which 1 were waited for; matrix products, arithmetic and copies ran while one was open for 2% of the time, Pallas kernels for 15%

profile of v1, /device:TPU:0, one launch (start us, length us, event | category | flops | bytes accessed | tf_op | source)
XLA Modules:
  0.0 197.4 jit_solution(1168193493208872919)
XLA Ops:
  7.2 0.9 copy.25
  8.1 0.1 eq.29
  8.2 0.1 eq.25
  8.4 0.7 broadcast_multiply_fusion
  9.1 0.6 reduce-window.6
  9.6 0.2 slice_reduce_fusion
  9.9 0.1 copy.24
  10.0 0.1 mul.286
  10.3 1.4 scatter_custom_fusion
  11.7 1.2 fusion.13
  12.9 1.2 fusion.15
  14.2 0.8 copy-done.5
  15.0 3.3 %gather_fusion = bf16[512,2048]{1,0:T(8,128)(2,1)} fusion(bf16[129,2048]{1,0:T(8,128)(2,1)S(1)} %concatenate.3, s32[1024]{0:T(1024)S(1)} %pad_clamp_fusion.1), kind=kCustom, calls=%fused_computation | custom fusion | bytes 4196352 | tf_op jit(solution)/shard_map/gather | solution.py:318
  18.4 55.6 %all_to_all.10 = bf16[8,64,2048]{2,1,0:T(8,128)(2,1)S(1)} all-to-all(bf16[8,64,2048]{2,1,0:T(8,128)(2,1)} %bitcast.42), channel_id=1, replica_groups=mesh['ep'=8,'tp'=4] {'ep'}, dimensions={0} | all-to-all | bytes 4194304 | tf_op jit(solution)/shard_map/all_to_all | solution.py:319
  74.0 2.3 %fusion.4 = f32[512,1024]{1,0:T(8,128)S(1)} fusion(bf16[512,2048]{1,0:T(8,128)(2,1)S(1)} %bitcast.43, bf16[1,2048,1024]{2,1,0:T(8,128)(2,1)S(1)} %copy-done.9), kind=kOutput, calls=%fused_computation.7 | convolution fusion | flops 2147483648 | bytes 8388608 | tf_op jit(solution)/shard_map/dot_general | solution.py:322
  76.4 3.5 %multiply_convert_fusion = bf16[512,1024]{1,0:T(8,128)(2,1)} fusion(f32[512,1024]{1,0:T(8,128)S(1)} %fusion.4, bf16[512,2048]{1,0:T(8,128)(2,1)S(1)} %bitcast.44, bf16[1,2048,1024]{2,1,0:T(8,128)(2,1)S(1)} %copy-done.10), kind=kOutput, calls=%fused_computation.9 | convolution fusion | flops 2150629376 | bytes 9437184 | tf_op jit(solution)/shard_map/dot_general | solution.py:323
  80.5 0.3 copy.21
  80.8 0.1 copy.22.shift_ref
  80.9 0.1 add_multiply_fusion
  81.1 50.5 %all-gather.2.cloned.1.call-done = bf16[512,4096]{1,0:T(8,128)(2,1)} async-done(((bf16[512,1024]{1,0:T(8,128)(2,1)}), bf16[512,4096]{1,0:T(8,128)(2,1)}) %all-gather.2.cloned.1.call-update) | async-done | bytes 4194320 | tf_op jit(solution)/shard_map/all_gather | solution.py:331
  131.6 6.6 %fusion.8 = bf16[512,512]{1,0:T(8,128)(2,1)} fusion(bf16[512,4096]{1,0:T(8,128)(2,1)} %all-gather.2.cloned.1.call-done, bf16[1,4096,512]{2,1,0:T(8,128)(2,1)} %param.28), kind=kOutput, calls=%fused_computation.12 | convolution fusion | flops 2147745792 | bytes 8912896 | tf_op jit(solution)/shard_map/dot_general | solution.py:330
  138.2 4.6 %all-to-all-start.1 = ((bf16[8,64,512]{2,1,0:T(8,128)(2,1)}), bf16[8,64,512]{2,1,0:T(8,128)(2,1)}, u32[]{:S(2)}, u32[]{:S(2)}) async-start(bf16[8,64,512]{2,1,0:T(8,128)(2,1)} %bitcast.45), calls=%async_computation.1 | async-start | bytes 1048576 | tf_op jit(solution)/shard_map/all_to_all | solution.py:341
  142.8 29.3 %mixer.1 = bf16[256,512]{1,0:T(8,128)(2,1)S(1)} custom-call(bf16[256,256]{1,0:T(8,128)(2,1)S(1)} %copy-done.3, f32[1,16]{1,0:T(1,128)S(1)} %bitcast.41, f32[256,16]{1,0:T(8,128)S(1)} %copy.22.shift_ref, bf16[2,1024,16]{2,1,0:T(8,128)(2,1)S(1)} %bitcast.39, f32[2,256,64]{2,1,0:T(8,128)S(1)} %bitcast.40, f32[4,1024]{1,0:T(4,128)S(1)} %pad_maximum_fusion.table_ref, ...), custom_call_target="tpu_custom_call" | custom-call | flops 20000000000 | bytes 10000000 | tf_op jit(solution)/shard_map/mixer/pallas_call | solution.py:244
  172.1 0.1 copy.23
  172.3 1.7 fusion.22
  174.0 1.7 fusion.12
  175.7 9.8 %all_gather.6 = bf16[128,1024]{1,0:T(8,128)(2,1)S(1)} all-gather(bf16[128,256]{1,0:T(8,128)(2,1)S(1)} %fusion.12), channel_id=1, replica_groups=mesh['ep'=8,'tp'=4] {'tp'}, dimensions={1}, use_global_device_ids=true | all-gather | bytes 327680 | tf_op jit(solution)/shard_map/all_gather | solution.py:337
  185.5 2.3 %gather_fusion.1 = bf16[256,512]{1,0:T(8,128)(2,1)S(1)} fusion(bf16[512,512]{1,0:T(8,128)(2,1)} %bitcast.13, s32[1024]{0:T(1024)S(1)} %pad_clamp_fusion), kind=kCustom, calls=%fused_computation.1 | custom fusion | bytes 525312 | tf_op jit(solution)/shard_map/gather | solution.py:348
  187.8 0.3 reshape.266
  188.2 0.7 multiply_reduce_fusion
  188.9 1.0 fusion.11
  189.8 0.7 copy.28
  (47 shorter events, 0.8 us)
Async XLA Ops:
  7.2 181.7 %copy-start = (bf16[1024,512]{1,0:T(8,128)(2,1)S(1)}, bf16[1024,512]{1,0:T(8,128)(2,1)}, u32[]{:S(2)}) copy-start(bf16[1024,512]{1,0:T(8,128)(2,1)} %param.31) | copy-start | bytes 3145732
  7.2 124.4 %all-gather.2.cloned.1.call-start = ((), (), s32[]{:S(2)}) async-start(), calls=%async_computation.2 | async-start | bytes 5242880 | tf_op jit(solution)/shard_map/all_gather | solution.py:331
  14.2 0.8 copy-start.5
  18.4 55.7 %copy-start.9 = (bf16[1,2048,1024]{2,1,0:T(8,128)(2,1)S(1)}, bf16[1,2048,1024]{2,1,0:T(8,128)(2,1)}, u32[]{:S(2)}) copy-start(bf16[1,2048,1024]{2,1,0:T(8,128)(2,1)} %param.26) | copy-start | bytes 12582916
  74.0 2.4 %copy-start.10 = (bf16[1,2048,1024]{2,1,0:T(8,128)(2,1)S(1)}, bf16[1,2048,1024]{2,1,0:T(8,128)(2,1)}, u32[]{:S(2)}) copy-start(bf16[1,2048,1024]{2,1,0:T(8,128)(2,1)} %param.27) | copy-start | bytes 12582916
  76.4 3.5 %copy-start.4 = (f32[16]{0:T(128)S(1)}, f32[16]{0:T(128)}, u32[]{:S(2)}) copy-start(f32[16]{0:T(128)} %param.17) | copy-start | bytes 196
  76.4 4.1 %copy-start.6 = (bf16[2,16,64,16]{2,3,1,0:T(8,128)(2,1)S(1)}, bf16[2,16,64,16]{2,3,1,0:T(8,128)(2,1)}, u32[]{:S(2)}) copy-start(bf16[2,16,64,16]{2,3,1,0:T(8,128)(2,1)} %param.19) | copy-start | bytes 196612
  76.4 4.4 %copy-start.7 = (f32[256,16]{0,1:T(8,128)S(1)}, f32[256,16]{0,1:T(8,128)}, u32[]{:S(2)}) copy-start(f32[256,16]{0,1:T(8,128)} %param.18) | copy-start | bytes 49156
  81.1 61.7 %copy-start.1 = (bf16[1024,512]{1,0:T(8,128)(2,1)S(1)}, bf16[1024,512]{1,0:T(8,128)(2,1)}, u32[]{:S(2)}) copy-start(bf16[1024,512]{1,0:T(8,128)(2,1)} %weight_ref.1) | copy-start | bytes 3145732
  81.1 61.7 %copy-start.2 = (f32[2,16,16,64]{3,2,1,0:T(8,128)S(1)}, f32[2,16,16,64]{3,2,1,0:T(8,128)}, u32[]{:S(2)}) copy-start(f32[2,16,16,64]{3,2,1,0:T(8,128)} %param.20) | copy-start | bytes 393220
  81.1 61.7 %copy-start.3 = (bf16[256,256]{1,0:T(8,128)(2,1)S(1)}, bf16[256,256]{1,0:T(8,128)(2,1)}, u32[]{:S(2)}) copy-start(bf16[256,256]{1,0:T(8,128)(2,1)} %x_ref.1) | copy-start | bytes 393220
  138.2 47.3 %all-to-all-start.1 = ((bf16[8,64,512]{2,1,0:T(8,128)(2,1)}), bf16[8,64,512]{2,1,0:T(8,128)(2,1)}, u32[]{:S(2)}, u32[]{:S(2)}) async-start(bf16[8,64,512]{2,1,0:T(8,128)(2,1)} %bitcast.45), calls=%async_computation.1 | async-start | bytes 1048576 | tf_op jit(solution)/shard_map/all_to_all | solution.py:341
  142.8 29.3 %copy-start.8 = (f32[128,2]{0,1:T(2,128)S(1)}, f32[128,2]{0,1:T(2,128)}, u32[]{:S(2)}) copy-start(f32[128,2]{0,1:T(2,128)} %param.25) | copy-start | bytes 3076
Sparse Core Ops, SparseCore 0:
  80.1 51.4 all-gather.1

commit v2 on v1

--- a/solution.py
+++ b/solution.py
@@ -157,17 +157,33 @@
     return dot(order, active).astype(jnp.bfloat16)
 
 
-def mixer_kernel(
+def remote(src, dst, send, recv, **target):
+    return pltpu.make_async_remote_copy(
+        src_ref=src, dst_ref=dst, send_sem=send, recv_sem=recv,
+        device_id=target, device_id_type=MESH,
+    )
+
+
+def fused_kernel(
     n_ep, n_tp, states,
     x_ref, rate_ref, shift_ref, map_ref, readout_ref, table_ref, weight_ref,
-    out_ref,
+    outgoing, gains, normed, sgate_ref, sup_ref, sdown_ref, gate_hbm, up_hbm, down_hbm,
+    out_ref, experts_ref,
     mag, push_re, push_im, pre, summary, active,
+    gate, up, down, arrived, hidden, result, returned, shared,
     ep_send, ep_recv, tp_send, tp_recv,
+    d_send, d_recv, h_send, h_recv, r_send, r_recv, s_send, s_recv, load,
 ):
     ep = lax.axis_index("ep")
     tp = lax.axis_index("tp")
     rows, channels = x_ref.shape
     merged = mag.shape[1]
+    cap, features = outgoing.shape[1:]
+    pair = hidden.shape[2] // cap
+    chips = n_ep // pair
+    chip = ep // pair
+    ff = gate.shape[1]
+    columns = down.shape[1]
     barrier = pltpu.get_barrier_semaphore()
     for d in range(1, n_ep):
         pl.semaphore_signal(
@@ -177,6 +193,18 @@
         pl.semaphore_signal(
             barrier, inc=1, device_id={"tp": lax.rem(tp + d, n_tp)}, device_id_type=MESH
         )
+    loads = [
+        pltpu.make_async_copy(hbm.at[0], vmem, load.at[i])
+        for i, (hbm, vmem) in enumerate(((gate_hbm, gate), (up_hbm, up), (down_hbm, down)))
+    ]
+    for copy in loads:
+        copy.start()
+    sends = []
+
+    def go(copy):
+        copy.start()
+        sends.append(copy)
+
     drive_into(x_ref, rate_ref, shift_ref, map_ref, table_ref, mag, push_re, push_im, states)
     zero = jnp.zeros((SUBLANES, merged), jnp.float32)
     ends_re, ends_im, product = sweep(table_ref, mag, push_re, push_im, zero, zero, False)
@@ -184,20 +212,36 @@
     for i, v in enumerate(end):
         summary[ep, i : i + 1, :] = v
     pl.semaphore_wait(barrier, n_ep + n_tp - 2)
-    copies = []
+    carries = []
     for d in range(1, n_ep):
-        copy = pltpu.make_async_remote_copy(
-            src_ref=summary.at[ep],
-            dst_ref=summary.at[ep],
-            send_sem=ep_send.at[d],
-            recv_sem=ep_recv.at[d],
-            device_id={"ep": lax.rem(ep + d, n_ep)},
-            device_id_type=MESH,
-        )
-        copy.start()
-        copies.append(copy)
-    for copy in copies:
-        copy.wait()
+        copy = remote(
+            summary.at[ep], summary.at[ep], ep_send.at[d], ep_recv.at[d],
+            ep=lax.rem(ep + d, n_ep),
+        )
+        go(copy)
+        carries.append(copy)
+    others = [pair * chip + lax.rem(ep + c, pair) for c in range(1, pair)]
+    for i in range(1, chips):
+        others += [pair * lax.rem(chip + i, chips) + c for c in range(pair)]
+    for target in others:
+        go(remote(
+            outgoing.at[target], arrived.at[ep], d_send.at[target], d_recv.at[ep], ep=target
+        ))
+    arrived[ep] = outgoing[ep]
+
+    tokens = normed[...]
+    v = dot(tokens, sgate_ref[...])
+    shared[tp] = (v / (1.0 + jnp.exp(-v)) * dot(tokens, sup_ref[...])).astype(jnp.bfloat16)
+    shares = []
+    for d in range(1, n_tp):
+        copy = remote(
+            shared.at[tp], shared.at[tp], s_send.at[d], s_recv.at[d], tp=lax.rem(tp + d, n_tp)
+        )
+        go(copy)
+        shares.append(copy)
+
+    for copy in carries:
+        copy.wait_recv()
 
     def fold(e, carry):
         part = summary[e]
@@ -209,71 +253,96 @@
     add_re, add_im = times(pre[2], pre[3], in_re, in_im)
     sweep(table_ref, mag, push_re, push_im, pre[0] + add_re, pre[1] + add_im, True)
     active[tp] = read_states(readout_ref, push_re, push_im, states)
-    copies = []
+    mixes = []
     for d in range(1, n_tp):
-        copy = pltpu.make_async_remote_copy(
-            src_ref=active.at[tp],
-            dst_ref=active.at[tp],
-            send_sem=tp_send.at[d],
-            recv_sem=tp_recv.at[d],
-            device_id={"tp": lax.rem(tp + d, n_tp)},
-            device_id_type=MESH,
-        )
-        copy.start()
-        copies.append(copy)
-    total = None
-    for d in range(n_tp):
-        if d > 0:
-            copies[d - 1].wait()
-        owner = lax.rem(tp + n_tp - d, n_tp)
-        at = pl.ds(pl.multiple_of(owner * channels, channels), channels)
-        part = dot(active[owner], weight_ref[at, :])
-        total = part if total is None else total + part
-    out_ref[...] = total.astype(out_ref.dtype)
-
-
-def mixer(mixer_input, log_step, decay_shift, input_map, readout, mixer_weight):
-    n_ep, n_tp = lax.axis_size("ep"), lax.axis_size("tp")
-    rows, channels = mixer_input.shape
-    groups = log_step.shape[0]
-    states, width = input_map.shape[2:]
-    merged = groups * states
-    _, cosine, sine, inject_re, inject_im = factors(log_step, states)
-    table = jnp.stack([a.reshape(merged) for a in (cosine, sine, inject_re, inject_im)])
-    f32 = jnp.float32
-    return pl.pallas_call(
-        functools.partial(mixer_kernel, n_ep, n_tp, states),
-        out_shape=jax.ShapeDtypeStruct((rows, mixer_weight.shape[1]), jnp.bfloat16),
-        in_specs=[pl.BlockSpec(memory_space=pltpu.VMEM)] * 7,
-        out_specs=pl.BlockSpec(memory_space=pltpu.VMEM),
-        scratch_shapes=[
-            pltpu.VMEM((rows, merged), f32),
-            pltpu.VMEM((rows, merged), f32),
-            pltpu.VMEM((rows, merged), f32),
-            pltpu.VMEM((4, SUBLANES, merged), f32),
-            pltpu.VMEM((n_ep, 4, merged), f32),
-            pltpu.VMEM((n_tp, rows, channels), jnp.bfloat16),
-            pltpu.SemaphoreType.DMA((n_ep,)),
-            pltpu.SemaphoreType.DMA((n_ep,)),
-            pltpu.SemaphoreType.DMA((n_tp,)),
-            pltpu.SemaphoreType.DMA((n_tp,)),
-        ],
-        compiler_params=pltpu.CompilerParams(
-            collective_id=0, has_side_effects=True, vmem_limit_bytes=40 * 1024 * 1024
-        ),
-        cost_estimate=pl.CostEstimate(
-            flops=20_000_000_000, bytes_accessed=10_000_000, transcendentals=0
-        ),
-        name="mixer",
-    )(
-        mixer_input,
-        log_step.reshape(1, groups),
-        decay_shift,
-        input_map.reshape(2, merged, width),
-        readout.reshape(2, channels, states),
-        table,
-        mixer_weight,
-    )
+        copy = remote(
+            active.at[tp], active.at[tp], tp_send.at[d], tp_recv.at[d], tp=lax.rem(tp + d, n_tp)
+        )
+        go(copy)
+        mixes.append(copy)
+    for copy in loads:
+        copy.wait()
+
+    def project(i):
+        there = lax.rem(chip + chips - i, chips)
+        for d in range(1, n_tp):
+            q = lax.rem(tp + d, n_tp)
+            remote(
+                hidden.at[there, q], hidden.at[there, q], h_send.at[there, q],
+                h_recv.at[there, q], tp=q,
+            ).wait_recv()
+        total = None
+        for q in range(n_tp):
+            part = dot(hidden[there, q], down[q * ff : (q + 1) * ff, :])
+            total = part if total is None else total + part
+        result[there] = total.astype(jnp.bfloat16).reshape(pair, cap, columns)
+        for c in range(pair):
+            if i == 0 and c == 0:
+                returned[ep] = result[there, lax.rem(ep, pair)]
+                continue
+            core = lax.rem(ep + c, pair) if i == 0 else c
+            target = pair * there + core
+            go(remote(
+                result.at[there, core], returned.at[ep], r_send.at[target], r_recv.at[ep],
+                ep=target,
+            ))
+
+    tile = min(ff, 256)
+    for i in range(chips):
+        there = lax.rem(chip + chips - i, chips)
+        for c in range(pair):
+            if i == 0 and c == 0:
+                continue
+            source = pair * there + (lax.rem(ep + c, pair) if i == 0 else c)
+            remote(
+                outgoing.at[source], arrived.at[source], d_send.at[source], d_recv.at[source],
+                ep=source,
+            ).wait_recv()
+        block = pl.ds(pair * there, pair)
+
+        @pl.loop(0, ff // tile)
+        def _(n):
+            at = pl.ds(pl.multiple_of(n * tile, tile), tile)
+            a = arrived[block].reshape(pair * cap, features)
+            v = dot(a, gate[:, at])
+            hidden[there, tp, :, at] = (
+                v / (1.0 + jnp.exp(-v)) * dot(a, up[:, at])
+            ).astype(jnp.bfloat16)
+
+        for d in range(1, n_tp):
+            q = lax.rem(tp + d, n_tp)
+            go(remote(
+                hidden.at[there, tp], hidden.at[there, tp], h_send.at[there, q],
+                h_recv.at[there, tp], tp=q,
+            ))
+        if i == 0:
+            for copy in mixes:
+                copy.wait_recv()
+            total = None
+            for q in range(n_tp):
+                part = dot(active[q], weight_ref[q * channels : (q + 1) * channels, :])
+                total = part if total is None else total + part
+            out_ref[...] = total.astype(out_ref.dtype)
+        else:
+            project(i - 1)
+    for copy in shares:
+        copy.wait_recv()
+    width = shared.shape[2]
+    common = None
+    for q in range(n_tp):
+        part = dot(shared[q], sdown_ref[q * width : (q + 1) * width, :])
+        common = part if common is None else common + part
+    project(chips - 1)
+    for source in others:
+        remote(
+            returned.at[source], returned.at[source], r_send.at[source], r_recv.at[source],
+            ep=source,
+        ).wait_recv()
+    back = returned[...].reshape(n_ep * cap, columns)
+    high, low = halves(gains[...])
+    experts_ref[...] = (common + (dot(high, back) + dot(low, back))).astype(experts_ref.dtype)
+    for copy in sends:
+        copy.wait_send()
 
 
 def shards(
@@ -294,62 +363,87 @@
     shared_up,
     shared_down,
 ):
-    mixer_out = mixer(mixer_input, log_step, decay_shift, input_map, readout, mixer_weight)
-    token_count = expert_input.shape[0]
-    features = expert_input.shape[1]
+    n_ep, n_tp = lax.axis_size("ep"), lax.axis_size("tp")
+    token_count, features = expert_input.shape
     top_count = routes.shape[1]
-    experts = lax.axis_size("ep")
-    capacity = 2 * token_count * top_count // experts
+    cap = 2 * token_count * top_count // n_ep
     values = expert_input.astype(jnp.float32)
     normed = (
         values * lax.rsqrt(jnp.mean(values * values, axis=-1, keepdims=True) + 1e-06) * norm_gain
     ).astype(jnp.bfloat16)
     flat_routes = routes.reshape(-1)
-    onehot = (flat_routes[:, None] == jnp.arange(experts, dtype=jnp.int32)[None, :]).astype(
-        jnp.int32
-    )
+    onehot = (flat_routes[:, None] == jnp.arange(n_ep, dtype=jnp.int32)[None, :]).astype(jnp.int32)
     before = jnp.sum((jnp.cumsum(onehot, axis=0) - onehot) * onehot, axis=1)
-    slot = flat_routes * capacity + before
-    owner = jnp.arange(flat_routes.shape[0], dtype=jnp.int32) // top_count
-    slot_token = jnp.full((experts * capacity,), token_count, jnp.int32).at[slot].set(owner)
-    slice_width = down_weight.shape[2]
-    received_rows = experts * capacity
-    padded = jnp.concatenate([normed, jnp.zeros((1, features), jnp.bfloat16)], axis=0)
-    outgoing = padded[slot_token].reshape(experts, capacity, features)
-    arrived = lax.all_to_all(outgoing, "ep", split_axis=0, concat_axis=0, tiled=True).reshape(
-        received_rows, features
-    )
-    gate_sum = jnp.dot(arrived, expert_switch_matrix[0], preferred_element_type=jnp.float32)
-    up_sum = jnp.dot(arrived, up_weight[0], preferred_element_type=jnp.float32)
-    expert_hidden = (jax.nn.silu(gate_sum) * up_sum).astype(jnp.bfloat16)
-    shared_hidden = (
-        jax.nn.silu(jnp.dot(normed, shared_gate, preferred_element_type=jnp.float32))
-        * jnp.dot(normed, shared_up, preferred_element_type=jnp.float32)
-    ).astype(jnp.bfloat16)
-    rows_here = down_weight[0]
-    routed_output = jnp.dot(
-        lax.all_gather(expert_hidden, "tp", axis=1, tiled=True),
-        rows_here,
-        preferred_element_type=jnp.float32,
-    )
-    rows_here = shared_down
-    common_contribution = jnp.dot(
-        lax.all_gather(shared_hidden, "tp", axis=1, tiled=True),
-        rows_here,
-        preferred_element_type=jnp.float32,
-    )
-    returned = lax.all_to_all(
-        routed_output.astype(jnp.bfloat16).reshape(experts, capacity, slice_width),
-        "ep",
-        split_axis=0,
-        concat_axis=0,
-        tiled=True,
-    ).reshape(received_rows, slice_width)
-    picked = returned[slot].reshape(token_count, top_count, slice_width).astype(jnp.float32)
-    experts_out = (common_contribution + jnp.sum(route_weight[:, :, None] * picked, axis=1)).astype(
-        jnp.bfloat16
-    )
-    return (mixer_out, experts_out)
+    slot = (flat_routes * cap + before).reshape(token_count, top_count)
+    hit = slot[:, :, None] == jnp.arange(n_ep * cap, dtype=jnp.int32)[None, None, :]
+    gains = jnp.sum(jnp.where(hit, route_weight[:, :, None], 0.0), axis=1)
+    chosen = jnp.any(hit, axis=1).astype(jnp.bfloat16)
+    outgoing = lax.dot_general(
+        chosen, normed, (((0,), (0,)), ((), ())), preferred_element_type=jnp.float32
+    ).astype(jnp.bfloat16).reshape(n_ep, cap, features)
+
+    rows, channels = mixer_input.shape
+    groups = log_step.shape[0]
+    states, width = input_map.shape[2:]
+    merged = groups * states
+    _, cosine, sine, inject_re, inject_im = factors(log_step, states)
+    table = jnp.stack([a.reshape(merged) for a in (cosine, sine, inject_re, inject_im)])
+    f32, bf16 = jnp.float32, jnp.bfloat16
+    pair = 2 if n_ep % 2 == 0 else 1
+    chips = n_ep // pair
+    ff = up_weight.shape[2]
+    depth, columns = down_weight.shape[1:]
+    vmem = pl.BlockSpec(memory_space=pltpu.VMEM)
+    dma = pltpu.SemaphoreType.DMA
+    return tuple(pl.pallas_call(
+        functools.partial(fused_kernel, n_ep, n_tp, states),
+        out_shape=(
+            jax.ShapeDtypeStruct((rows, mixer_weight.shape[1]), bf16),
+            jax.ShapeDtypeStruct((token_count, columns), bf16),
+        ),
+        in_specs=[vmem] * 13 + [pl.BlockSpec(memory_space=pl.ANY)] * 3,
+        out_specs=(vmem, vmem),
+        scratch_shapes=[
+            pltpu.VMEM((rows, merged), f32),
+            pltpu.VMEM((rows, merged), f32),
+            pltpu.VMEM((rows, merged), f32),
+            pltpu.VMEM((4, SUBLANES, merged), f32),
+            pltpu.VMEM((n_ep, 4, merged), f32),
+            pltpu.VMEM((n_tp, rows, channels), bf16),
+            pltpu.VMEM((features, ff), bf16),
+            pltpu.VMEM((features, ff), bf16),
+            pltpu.VMEM((depth, columns), bf16),
+            pltpu.VMEM((n_ep, cap, features), bf16),
+            pltpu.VMEM((chips, n_tp, pair * cap, ff), bf16),
+            pltpu.VMEM((chips, pair, cap, columns), bf16),
+            pltpu.VMEM((n_ep, cap, columns), bf16),
+            pltpu.VMEM((n_tp, token_count, shared_up.shape[1]), bf16),
+            dma((n_ep,)), dma((n_ep,)), dma((n_tp,)), dma((n_tp,)),
+            dma((n_ep,)), dma((n_ep,)), dma((chips, n_tp)), dma((chips, n_tp)),
+            dma((n_ep,)), dma((n_ep,)), dma((n_tp,)), dma((n_tp,)), dma((3,)),
+        ],
+        compiler_params=pltpu.CompilerParams(
+            collective_id=0, has_side_effects=True, vmem_limit_bytes=56 * 1024 * 1024
+        ),
+        name="fused",
+    )(
+        mixer_input,
+        log_step.reshape(1, groups),
+        decay_shift,
+        input_map.reshape(2, merged, width),
+        readout.reshape(2, channels, states),
+        table,
+        mixer_weight,
+        outgoing,
+        gains,
+        normed,
+        shared_gate,
+        shared_up,
+        shared_down,
+        expert_switch_matrix,
+        up_weight,
+        down_weight,
+    ))
 
 
 def solution(mesh):

time: 198 us -> 116 us (0.59)
  the two profiles are of different devices: /device:TPU:0 before, /device:TPU:21 now
where the time goes in v2:
time: 116 us; the launch traced here: 115 us
  Pallas kernels  96.8 us (83%)
  local copies, waits for them, and re-layouts  8.72 us (8%)
  other arithmetic  7.01 us (6%)
  matrix products  2.11 us (2%)
    pallas_call x1, Pallas kernels, shards(): pl.pallas_call(functools.partial(fused_kernel, n_ep, n_tp, states), out_s...  96.8 us
    unnamed x7, local copies, waits for them, and re-layouts  7.56 us

profile of v2, /device:TPU:21, one launch (start us, length us, event | category | flops | bytes accessed | tf_op | source)
XLA Modules:
  0.0 115.4 jit_solution(17376001036667846587)
XLA Ops:
  0.6 1.2 %fusion = f32[128]{0:T(128)S(1)} fusion(bf16[128,2048]{1,0:T(8,128)(2,1)} %param.22), kind=kLoop, calls=%fused_computation.3 | loop fusion | flops 786304 | bytes 524800 | tf_op jit(solution)/shard_map/reduce_sum | solution.py:372
  1.9 0.7 fusion.7
  2.6 0.1 mul.225
  2.6 0.1 mul.226
  2.7 0.1 mul.241
  2.8 0.1 mul.230
  2.9 0.1 mul.233
  2.9 0.1 mul.234
  3.0 0.2 add_multiply_fusion
  3.2 0.6 pad_maximum_fusion.table_ref
  3.8 0.8 copy.37
  4.6 0.1 eq.42
  4.7 0.1 eq.38
  4.9 0.6 reduce-window.6
  5.5 0.2 slice_reduce_fusion
  5.7 0.1 fusion.5
  5.8 0.1 reduce_sum.30
  6.0 0.1 copy.39
  6.0 0.7 multiply_add_fusion.1
  6.7 0.1 fusion.3
  6.9 1.5 %copy.40.shift_ref = f32[256,16]{1,0:T(8,128)} copy(f32[256,16]{0,1:T(8,128)} %param.18) | data formatting | bytes 32768 | tf_op args[2]
  8.3 1.5 %select_reduce_fusion.gains = f32[128,512]{1,0:T(8,128)} fusion(f32[128,2]{0,1:T(2,128)} %param.25, s32[128,2]{0,1:T(2,128)S(1)} %multiply_add_fusion.1), kind=kLoop, calls=%fused_computation.6 | loop fusion | flops 327680 | bytes 264192 | tf_op jit(solution)/shard_map/reduce_sum | solution.py:379
  9.9 1.2 %fusion.2.normed = bf16[128,2048]{1,0:T(8,128)(2,1)S(1)} fusion(bf16[128,2048]{1,0:T(8,128)(2,1)} %param.22, f32[2048]{0:T(1024)} %param.23, f32[128]{0:T(128)S(1)} %add_rsqrt_fusion), kind=kLoop, calls=%fused_computation.5 | loop fusion | flops 1048576 | bytes 1057280 | tf_op jit(solution)/shard_map/convert_element_type | solution.py:373
  11.1 0.0 copy-start
  11.1 2.1 %copy.36 = bf16[2,16,64,16]{3,2,1,0:T(8,128)(2,1)} copy(bf16[2,16,64,16]{2,3,1,0:T(8,128)(2,1)} %param.19) | data formatting | bytes 131072 | tf_op args[3]
  13.2 2.1 %convolution_convert_fusion = bf16[512,2048]{1,0:T(8,128)(2,1)} fusion(pred[128,512]{1,0:T(8,128)(4,1)S(1)} %fusion.3, bf16[128,2048]{1,0:T(8,128)(2,1)S(1)} %fusion.2.normed), kind=kOutput, calls=%fused_computation | convolution fusion | flops 269484032 | bytes 2686976 | tf_op jit(solution)/shard_map/dot_general | solution.py:381
  15.3 0.0 copy-done
  15.3 96.8 %fused.1 = (bf16[256,512]{1,0:T(8,128)(2,1)}, bf16[128,512]{1,0:T(8,128)(2,1)}) custom-call(bf16[256,256]{1,0:T(8,128)(2,1)} %x_ref.1, f32[1,16]{1,0:T(1,128)} %bitcast.17, f32[256,16]{1,0:T(8,128)} %copy.40.shift_ref, bf16[2,1024,16]{2,1,0:T(8,128)(2,1)} %bitcast.15, f32[2,256,64]{2,1,0:T(8,128)} %bitcast.16, f32[4,1024]{1,0:T(4,128)} %pad_maximum_fusion.table_ref, ...), custom_call_target="tpu_custom_call" | custom-call | tf_op jit(solution)/shard_map/fused/pallas_call | solution.py:398
  112.1 1.7 %copy.43 = bf16[256,512]{1,0:T(8,128)(2,1)} copy(bf16[256,512]{1,0:T(8,128)(2,1)} %get-tuple-element.10) | data formatting | bytes 524288
  113.8 1.6 %copy.44 = bf16[128,512]{1,0:T(8,128)(2,1)} copy(bf16[128,512]{1,0:T(8,128)(2,1)} %get-tuple-element.11) | data formatting | bytes 262144
  (8 shorter events, 0.1 us)
Async XLA Ops:
  11.1 4.2 %copy-start = (bf16[128,2048]{1,0:T(8,128)(2,1)}, bf16[128,2048]{1,0:T(8,128)(2,1)S(1)}, u32[]{:S(2)}) copy-start(bf16[128,2048]{1,0:T(8,128)(2,1)S(1)} %fusion.2.normed) | copy-start | bytes 1572868

commit v3 on v2

--- a/solution.py
+++ b/solution.py
@@ -205,13 +205,25 @@
         copy.start()
         sends.append(copy)
 
+    pl.semaphore_wait(barrier, n_ep + n_tp - 2)
+    others = [pair * chip + lax.rem(ep + c, pair) for c in range(1, pair)]
+    for i in range(1, chips):
+        others += [pair * lax.rem(chip + i, chips) + c for c in range(pair)]
+
+    def dispatch(targets):
+        for target in targets:
+            go(remote(
+                outgoing.at[target], arrived.at[ep], d_send.at[target], d_recv.at[ep], ep=target
+            ))
+
+    first = 2 * pair - 1
+    dispatch(others[:first])
     drive_into(x_ref, rate_ref, shift_ref, map_ref, table_ref, mag, push_re, push_im, states)
     zero = jnp.zeros((SUBLANES, merged), jnp.float32)
     ends_re, ends_im, product = sweep(table_ref, mag, push_re, push_im, zero, zero, False)
     end = join(table_ref, ends_re, ends_im, product, pre, rows // SUBLANES)
     for i, v in enumerate(end):
         summary[ep, i : i + 1, :] = v
-    pl.semaphore_wait(barrier, n_ep + n_tp - 2)
     carries = []
     for d in range(1, n_ep):
         copy = remote(
@@ -220,13 +232,7 @@
         )
         go(copy)
         carries.append(copy)
-    others = [pair * chip + lax.rem(ep + c, pair) for c in range(1, pair)]
-    for i in range(1, chips):
-        others += [pair * lax.rem(chip + i, chips) + c for c in range(pair)]
-    for target in others:
-        go(remote(
-            outgoing.at[target], arrived.at[ep], d_send.at[target], d_recv.at[ep], ep=target
-        ))
+    dispatch(others[first:])
     arrived[ep] = outgoing[ep]
 
     tokens = normed[...]
@@ -240,6 +246,39 @@
         go(copy)
         shares.append(copy)
 
+    tile = min(ff, 256)
+
+    def expand(i):
+        there = lax.rem(chip + chips - i, chips)
+        for c in range(pair):
+            if i == 0 and c == 0:
+                continue
+            source = pair * there + (lax.rem(ep + c, pair) if i == 0 else c)
+            remote(
+                outgoing.at[source], arrived.at[source], d_send.at[source], d_recv.at[source],
+                ep=source,
+            ).wait_recv()
+        block = pl.ds(pair * there, pair)
+
+        @pl.loop(0, ff // tile)
+        def _(n):
+            at = pl.ds(pl.multiple_of(n * tile, tile), tile)
+            a = arrived[block].reshape(pair * cap, features)
+            v = dot(a, gate[:, at])
+            hidden[there, tp, :, at] = (
+                v / (1.0 + jnp.exp(-v)) * dot(a, up[:, at])
+            ).astype(jnp.bfloat16)
+
+        for d in range(1, n_tp):
+            q = lax.rem(tp + d, n_tp)
+            go(remote(
+                hidden.at[there, tp], hidden.at[there, tp], h_send.at[there, q],
+                h_recv.at[there, tp], tp=q,
+            ))
+
+    for copy in loads[:2]:
+        copy.wait()
+    expand(0)
     for copy in carries:
         copy.wait_recv()
 
@@ -260,9 +299,6 @@
         )
         go(copy)
         mixes.append(copy)
-    for copy in loads:
-        copy.wait()
-
     def project(i):
         there = lax.rem(chip + chips - i, chips)
         for d in range(1, n_tp):
@@ -287,44 +323,18 @@
                 ep=target,
             ))
 
-    tile = min(ff, 256)
-    for i in range(chips):
-        there = lax.rem(chip + chips - i, chips)
-        for c in range(pair):
-            if i == 0 and c == 0:
-                continue
-            source = pair * there + (lax.rem(ep + c, pair) if i == 0 else c)
-            remote(
-                outgoing.at[source], arrived.at[source], d_send.at[source], d_recv.at[source],
-                ep=source,
-            ).wait_recv()
-        block = pl.ds(pair * there, pair)
-
-        @pl.loop(0, ff // tile)
-        def _(n):
-            at = pl.ds(pl.multiple_of(n * tile, tile), tile)
-            a = arrived[block].reshape(pair * cap, features)
-            v = dot(a, gate[:, at])
-            hidden[there, tp, :, at] = (
-                v / (1.0 + jnp.exp(-v)) * dot(a, up[:, at])
-            ).astype(jnp.bfloat16)
-
-        for d in range(1, n_tp):
-            q = lax.rem(tp + d, n_tp)
-            go(remote(
-                hidden.at[there, tp], hidden.at[there, tp], h_send.at[there, q],
-                h_recv.at[there, tp], tp=q,
-            ))
-        if i == 0:
-            for copy in mixes:
-                copy.wait_recv()
-            total = None
-            for q in range(n_tp):
-                part = dot(active[q], weight_ref[q * channels : (q + 1) * channels, :])
-                total = part if total is None else total + part
-            out_ref[...] = total.astype(out_ref.dtype)
-        else:
-            project(i - 1)
+    for copy in loads[2:]:
+        copy.wait()
+    for i in range(1, chips):
+        expand(i)
+        project(i - 1)
+    for copy in mixes:
+        copy.wait_recv()
+    total = None
+    for q in range(n_tp):
+        part = dot(active[q], weight_ref[q * channels : (q + 1) * channels, :])
+        total = part if total is None else total + part
+    out_ref[...] = total.astype(out_ref.dtype)
     for copy in shares:
         copy.wait_recv()
     width = shared.shape[2]

time: 116 us -> 110 us (0.948)
  the two profiles are of different devices: /device:TPU:21 before, /device:TPU:0 now
where the time goes in v3:
time: 110 us; the launch traced here: 109 us
  Pallas kernels  90.5 us (82%)
  local copies, waits for them, and re-layouts  8.72 us (8%)
  other arithmetic  7.01 us (6%)
  matrix products  2.11 us (2%)
    pallas_call x1, Pallas kernels, shards(): pl.pallas_call(functools.partial(fused_kernel, n_ep, n_tp, states), out_s...  90.5 us
    unnamed x7, local copies, waits for them, and re-layouts  7.56 us

profile of v3, /device:TPU:0, one launch (start us, length us, event | category | flops | bytes accessed | tf_op | source)
XLA Modules:
  0.0 109.0 jit_solution(12654188588584079122)
XLA Ops:
  0.6 1.2 %fusion = f32[128]{0:T(128)S(1)} fusion(bf16[128,2048]{1,0:T(8,128)(2,1)} %param.22), kind=kLoop, calls=%fused_computation.3 | loop fusion | flops 786304 | bytes 524800 | tf_op jit(solution)/shard_map/reduce_sum | solution.py:382
  1.9 0.7 fusion.7
  2.6 0.1 mul.225
  2.6 0.1 mul.226
  2.7 0.1 mul.241
  2.8 0.1 mul.230
  2.9 0.1 mul.233
  2.9 0.1 mul.234
  3.0 0.2 add_multiply_fusion
  3.2 0.6 pad_maximum_fusion.table_ref
  3.8 0.8 copy.37
  4.6 0.1 eq.42
  4.7 0.1 eq.38
  4.9 0.6 reduce-window.6
  5.5 0.2 slice_reduce_fusion
  5.7 0.1 fusion.5
  5.8 0.1 reduce_sum.30
  6.0 0.1 copy.39
  6.0 0.7 multiply_add_fusion.1
  6.7 0.1 fusion.3
  6.9 1.5 %copy.40.shift_ref = f32[256,16]{1,0:T(8,128)} copy(f32[256,16]{0,1:T(8,128)} %param.18) | data formatting | bytes 32768 | tf_op args[2]
  8.3 1.5 %select_reduce_fusion.gains = f32[128,512]{1,0:T(8,128)} fusion(f32[128,2]{0,1:T(2,128)} %param.25, s32[128,2]{0,1:T(2,128)S(1)} %multiply_add_fusion.1), kind=kLoop, calls=%fused_computation.6 | loop fusion | flops 327680 | bytes 264192 | tf_op jit(solution)/shard_map/reduce_sum | solution.py:389
  9.9 1.2 %fusion.2.normed = bf16[128,2048]{1,0:T(8,128)(2,1)S(1)} fusion(bf16[128,2048]{1,0:T(8,128)(2,1)} %param.22, f32[2048]{0:T(1024)} %param.23, f32[128]{0:T(128)S(1)} %add_rsqrt_fusion), kind=kLoop, calls=%fused_computation.5 | loop fusion | flops 1048576 | bytes 1057280 | tf_op jit(solution)/shard_map/convert_element_type | solution.py:383
  11.1 0.0 copy-start
  11.1 2.1 %copy.36 = bf16[2,16,64,16]{3,2,1,0:T(8,128)(2,1)} copy(bf16[2,16,64,16]{2,3,1,0:T(8,128)(2,1)} %param.19) | data formatting | bytes 131072 | tf_op args[3]
  13.2 2.1 %convolution_convert_fusion = bf16[512,2048]{1,0:T(8,128)(2,1)} fusion(pred[128,512]{1,0:T(8,128)(4,1)S(1)} %fusion.3, bf16[128,2048]{1,0:T(8,128)(2,1)S(1)} %fusion.2.normed), kind=kOutput, calls=%fused_computation | convolution fusion | flops 269484032 | bytes 2686976 | tf_op jit(solution)/shard_map/dot_general | solution.py:391
  15.3 0.0 copy-done
  15.3 90.5 %fused.1 = (bf16[256,512]{1,0:T(8,128)(2,1)}, bf16[128,512]{1,0:T(8,128)(2,1)}) custom-call(bf16[256,256]{1,0:T(8,128)(2,1)} %x_ref.1, f32[1,16]{1,0:T(1,128)} %bitcast.17, f32[256,16]{1,0:T(8,128)} %copy.40.shift_ref, bf16[2,1024,16]{2,1,0:T(8,128)(2,1)} %bitcast.15, f32[2,256,64]{2,1,0:T(8,128)} %bitcast.16, f32[4,1024]{1,0:T(4,128)} %pad_maximum_fusion.table_ref, ...), custom_call_target="tpu_custom_call" | custom-call | tf_op jit(solution)/shard_map/fused/pallas_call | solution.py:408
  105.8 1.7 %copy.43 = bf16[256,512]{1,0:T(8,128)(2,1)} copy(bf16[256,512]{1,0:T(8,128)(2,1)} %get-tuple-element.10) | data formatting | bytes 524288
  107.5 1.6 %copy.44 = bf16[128,512]{1,0:T(8,128)(2,1)} copy(bf16[128,512]{1,0:T(8,128)(2,1)} %get-tuple-element.11) | data formatting | bytes 262144
  (8 shorter events, 0.1 us)
Async XLA Ops:
  11.1 4.2 %copy-start = (bf16[128,2048]{1,0:T(8,128)(2,1)}, bf16[128,2048]{1,0:T(8,128)(2,1)S(1)}, u32[]{:S(2)}) copy-start(bf16[128,2048]{1,0:T(8,128)(2,1)S(1)} %fusion.2.normed) | copy-start | bytes 1572868
